TPU v7x, 32 devices: a whole 2x2x4 slice. The times are simulated.
32 devices in a mesh: sp: 16 (over z, y, x), tp: 2 (over core).
Axes of the slice: x: 2, y: 2, z: 4, core: 2. Of those that a mesh axis runs over, the one named last changes fastest.
Arguments:
- tokens: bfloat16 [2048, 2048], P(('sp', 'tp')), may hold values from -6 to 6
- input_norm_gain: float32 [2048], replicated, may hold values from 0.1 to 1.9
- differential_query: bfloat16 [2048, 1024], P(None, 'tp'), may hold values from -0.176776695 to 0.176776695, as said below
- differential_key: bfloat16 [2048, 1024], P(None, 'tp'), may hold values from -0.176776695 to 0.176776695, as said below
- differential_value: bfloat16 [2048, 1024], P(None, 'tp'), may hold values from -0.125 to 0.125
- query_norm_gain: float32 [64], replicated, may hold values from 1.15 to 5
- key_norm_gain: float32 [64], replicated, may hold values from 1.15 to 5
- second_map_weight: float32 [8], P('tp'), may hold values from 0.3 to 0.8
- differential_norm_gain: float32 [128], replicated, may hold values from 0.1 to 1.9
- linear_query: bfloat16 [2048, 512], P(None, 'tp'), may hold values from -0.125 to 0.125
- linear_key: bfloat16 [2048, 512], P(None, 'tp'), may hold values from -0.125 to 0.125
- linear_value: bfloat16 [2048, 1024], P(None, 'tp'), may hold values from -0.125 to 0.125
- linear_output_gate: bfloat16 [2048, 1024], P(None, 'tp'), may hold values from -0.125 to 0.125
- forget_down_factor: bfloat16 [2048, 32], replicated, may hold values from -0.125 to 0.125
- forget_up_factor: bfloat16 [32, 512], P(None, 'tp'), may hold values from -2.109375 to 2.109375
- forget_bias: float32 [512], P('tp'), may hold values from -0.5 to 10
- extra_shrinkage_exponent: float32 [2048, 8], P('sp', 'tp'), may hold values from -1.5 to 0
- linear_norm_gain: float32 [128], replicated, may hold values from 0.1 to 1.9
- differential_output_rows: bfloat16 [1024, 2048], P('tp'), may hold values from -0.125 to 0.125
- linear_output_rows: bfloat16 [1024, 2048], P('tp'), may hold values from -0.125 to 0.125
Outputs:
- layer_out: bfloat16 [2048, 2048], P(('sp', 'tp'))
Inputs may be any that keep to these rules, and one draw needn't show every extreme that they name: `differential_query`: independent entries of scale one over sqrt(2048). `differential_key`: entries of scale one over sqrt(2048).
All inputs are finite; a program needn't handle non-finite values.
Results may differ from a plain program's by a relative error of at most 0.015.
Values may be sent and summed in bfloat16 or wider, within the bound.
A program may use at most 64 MiB of HBM per device.

v0:
```python
from functools import partial

import jax
import jax.numpy as jnp
from jax import lax
from jax.sharding import PartitionSpec as P

HEAD = 64
VDIM = 128
RECURRENT_DIM = 64
GLA_DV = 128
BLOCK = 64


RMS_EPS = 1e-06
SOFTMAX_DIVISOR = 16.0
OUT_SCALE = 0.8
NEG_LARGE = -1e30
HIGHEST = lax.Precision.HIGHEST


def partner(block, axis, apart):
    count = lax.axis_size(axis)
    route = []
    for low in range(count):
        high = low | 1 << apart
        if high != low and high < count:
            route += [(low, high), (high, low)]
    return lax.ppermute(block, axis, route)


def prefix(shard, axis, combine, identity):
    devices, position = (lax.axis_size(axis), lax.axis_index(axis))
    everything = jax.tree.map(lambda part: lax.all_gather(part, axis), shard)
    start = jax.tree.map(
        lambda part, zero: jnp.broadcast_to(jnp.asarray(zero, part.dtype), part.shape),
        shard,
        identity,
    )

    def turn(k, before):
        reached = k < position
        new = combine(before, jax.tree.map(lambda part: part[k], everything))
        return jax.tree.map(lambda a, b: jnp.where(reached, a, b), new, before)

    return lax.fori_loop(0, devices, turn, start)


def rms_scale(values, scale_gain):
    mean_sq = jnp.mean(values * values, axis=-1, keepdims=True)
    return values * lax.rsqrt(mean_sq + RMS_EPS) * scale_gain


def block_length(total_rows, shard_rows):
    best = shard_rows
    shard_total = total_rows // shard_rows
    for multiple in range(1, shard_total + 1):
        if shard_total % multiple == 0 and shard_rows * multiple <= 2048:
            best = shard_rows * multiple
    return best


def combine_chain(earlier, later):
    return (earlier[0] * later[0], earlier[1] * later[0][..., None] + later[1])


def keep_carry(carry_now):
    return carry_now


def attend_span(query_set, query_pos, keys_here, values_here, key_pos, carry_now):
    row_peaks, totals, numerators = carry_now
    query_rows = query_set.shape[0]
    group_count = query_set.shape[1]
    attn_heads = group_count // 2
    span_rows = keys_here.shape[0]
    scores = jnp.einsum(
        "tgd,kgd->gtk", query_set, keys_here, preferred_element_type=jnp.float32
    ) * HEAD ** (-0.5)
    causal = key_pos[None, :] <= query_pos[:, None]
    scores = jnp.where(causal[None], scores, NEG_LARGE)
    new_peaks = jnp.maximum(row_peaks, jnp.max(scores, axis=-1))
    weights = jnp.where(causal[None], jnp.exp(scores - new_peaks[..., None]), 0.0)
    factor = jnp.exp(row_peaks - new_peaks)
    totals = totals * factor + jnp.sum(weights, axis=-1)
    rounded = weights.astype(jnp.bfloat16).reshape(attn_heads, 2, query_rows, span_rows)
    contrib = jnp.einsum(
        "hmtk,khv->hmtv", rounded, values_here, preferred_element_type=jnp.float32
    ).reshape(group_count, query_rows, VDIM)
    return (new_peaks, totals, numerators * factor[..., None] + contrib)


def per_device(
    tokens,
    input_norm_gain,
    differential_query,
    differential_key,
    differential_value,
    query_norm_gain,
    key_norm_gain,
    second_map_weight,
    differential_norm_gain,
    linear_query,
    linear_key,
    linear_value,
    linear_output_gate,
    forget_down_factor,
    forget_up_factor,
    forget_bias,
    extra_shrinkage_exponent,
    linear_norm_gain,
    differential_output_rows,
    linear_output_rows,
):
    sp_size = lax.axis_size("sp")
    sp_index = lax.axis_index("sp")
    attn_heads = second_map_weight.shape[0]
    linear_head_list = extra_shrinkage_exponent.shape[1]
    normed = rms_scale(tokens.astype(jnp.float32), input_norm_gain).astype(jnp.bfloat16)
    parts_list = [
        differential_query,
        differential_key,
        differential_value,
        linear_query,
        linear_key,
        linear_value,
        linear_output_gate,
        forget_down_factor,
    ]
    packed = jnp.concatenate(parts_list, axis=1)
    bounds = [0]
    for matrix in parts_list:
        bounds.append(bounds[-1] + matrix.shape[1])
    projected = jnp.dot(
        lax.all_gather(normed, "tp", axis=0, tiled=True), packed, preferred_element_type=jnp.float32
    ).astype(jnp.bfloat16)
    row_count = projected.shape[0]
    half_rows = row_count // 2
    bit_count = sp_size.bit_length() - 1

    def section(column_set):
        return projected[:, bounds[column_set] : bounds[column_set + 1]]

    group_count = 2 * attn_heads
    query_norm = rms_scale(
        section(0).astype(jnp.float32).reshape(row_count, group_count, HEAD), query_norm_gain
    ).astype(jnp.bfloat16)
    key_norm = rms_scale(
        section(1).astype(jnp.float32).reshape(row_count, group_count, HEAD), key_norm_gain
    ).astype(jnp.bfloat16)
    key_flat = key_norm.reshape(row_count, group_count * HEAD)
    value_flat = section(2)
    far_queries = query_norm[half_rows:].reshape(half_rows, group_count * HEAD)
    for bit in range(bit_count):
        far_queries = partner(far_queries, "sp", bit)
    mirror_index = sp_size - 1 - sp_index
    own_pos = sp_index * row_count + jnp.arange(half_rows, dtype=jnp.int32)
    far_pos = mirror_index * row_count + half_rows + jnp.arange(half_rows, dtype=jnp.int32)
    query_sets = [
        (query_norm[:half_rows], own_pos),
        (far_queries.reshape(half_rows, group_count, HEAD), far_pos),
    ]
    fold_start = tuple(
        (
            (
                jnp.full((group_count, query_set.shape[0]), NEG_LARGE, jnp.float32),
                jnp.zeros((group_count, query_set.shape[0]), jnp.float32),
                jnp.zeros((group_count, query_set.shape[0], VDIM), jnp.float32),
            )
            for query_set, query_pos in query_sets
        )
    )
    key_rows = lax.all_gather(key_flat, "sp", axis=0, tiled=True)
    value_rows = lax.all_gather(value_flat, "sp", axis=0, tiled=True)
    piece_rows = key_rows.shape[0]
    span_rows = block_length(piece_rows, row_count)

    def attend(span_index, carries):
        row_start = span_index * span_rows
        keys_here = lax.dynamic_slice_in_dim(
            key_rows, span_index * span_rows, span_rows, 0
        ).reshape(span_rows, group_count, HEAD)
        values_here = lax.dynamic_slice_in_dim(
            value_rows, span_index * span_rows, span_rows, 0
        ).reshape(span_rows, attn_heads, VDIM)
        key_pos = row_start + jnp.arange(span_rows, dtype=jnp.int32)
        results = []
        for (query_set, query_pos), carry_in in zip(query_sets, carries):
            work = partial(attend_span, query_set, query_pos, keys_here, values_here, key_pos)
            results.append(lax.cond(row_start <= jnp.max(query_pos), work, keep_carry, carry_in))
        return tuple(results)

    folded = lax.fori_loop(0, piece_rows // span_rows, attend, fold_start)

    def finish(carry_set):
        row_peaks, totals, numerators = carry_set
        set_rows = totals.shape[1]
        maps_out = (numerators / totals[..., None]).reshape(attn_heads, 2, set_rows, VDIM)
        attn_mix = maps_out[:, 0] - second_map_weight[:, None, None] * maps_out[:, 1]
        return (
            (rms_scale(attn_mix, differential_norm_gain) * OUT_SCALE)
            .transpose(1, 0, 2)
            .reshape(set_rows, attn_heads * VDIM)
            .astype(jnp.bfloat16)
        )

    own_rows = finish(folded[0])
    far_rows = finish(folded[1])
    for bit in range(bit_count):
        far_rows = partner(far_rows, "sp", bit)
    attn_out = jnp.concatenate([own_rows, far_rows], axis=0)
    chain_queries = section(3).astype(jnp.float32).reshape(
        row_count, linear_head_list, RECURRENT_DIM
    ) * RECURRENT_DIM ** (-0.5)
    chain_keys = section(4).astype(jnp.float32).reshape(row_count, linear_head_list, RECURRENT_DIM)
    chain_values = section(5).astype(jnp.float32).reshape(row_count, linear_head_list, GLA_DV)
    gated = jax.nn.silu(section(6).astype(jnp.float32)).reshape(row_count, linear_head_list, GLA_DV)
    sigmoid_preactivation = (
        jnp.dot(section(7), forget_up_factor, preferred_element_type=jnp.float32) + forget_bias
    )
    shrinkage_exponent = (
        jax.nn.log_sigmoid(sigmoid_preactivation).reshape(
            row_count, linear_head_list, RECURRENT_DIM
        )
        / SOFTMAX_DIVISOR
        + extra_shrinkage_exponent[:, :, None]
    )
    block_total = row_count // BLOCK

    def blockify(array):
        return array.reshape(block_total, BLOCK, linear_head_list, array.shape[-1])

    causal_block = jnp.arange(BLOCK)[:, None] >= jnp.arange(BLOCK)[None, :]

    def chain_block(carry, inputs):
        carried, log_total = carry
        query_block, key_block, value_block, decay_block = inputs
        log_cum = jnp.cumsum(decay_block, axis=0)
        log_last = log_cum[-1]
        query_decayed = query_block * jnp.exp(log_cum)
        key_inverse = key_block * jnp.exp(-log_cum)
        inner_scores = jnp.einsum("thd,shd->hts", query_decayed, key_inverse, precision=HIGHEST)
        inner_scores = jnp.where(causal_block[None], inner_scores, 0.0)
        local_out = jnp.einsum("hts,she->the", inner_scores, value_block, precision=HIGHEST)
        local_out = local_out + jnp.einsum(
            "thd,hde->the", query_decayed, carried, precision=HIGHEST
        )
        key_end = key_block * jnp.exp(log_last[None] - log_cum)
        carried = carried * jnp.exp(log_last)[..., None] + jnp.einsum(
            "thd,the->hde", key_end, value_block, precision=HIGHEST
        )
        carried_query = query_decayed * jnp.exp(log_total)[None]
        return ((carried, log_total + log_last), (local_out, carried_query))

    chain_zero = (
        jnp.zeros((linear_head_list, RECURRENT_DIM, GLA_DV), jnp.float32),
        jnp.zeros((linear_head_list, RECURRENT_DIM), jnp.float32),
    )
    (own_state, log_total), (local_out, carried_query) = lax.scan(
        chain_block,
        chain_zero,
        (
            blockify(chain_queries),
            blockify(chain_keys),
            blockify(chain_values),
            blockify(shrinkage_exponent),
        ),
    )
    local_out = local_out.reshape(row_count, linear_head_list, GLA_DV)
    carried_query = carried_query.reshape(row_count, linear_head_list, RECURRENT_DIM)
    own_decay = jnp.exp(log_total)
    carried_in = prefix(
        (own_decay, own_state),
        "sp",
        combine_chain,
        (jnp.ones_like(own_decay), jnp.zeros_like(own_state)),
    )[1]
    chain_full = local_out + jnp.einsum(
        "thd,hde->the", carried_query, carried_in, precision=HIGHEST
    )
    chain_out = (
        (rms_scale(chain_full, linear_norm_gain) * gated)
        .reshape(row_count, linear_head_list * GLA_DV)
        .astype(jnp.bfloat16)
    )
    return lax.psum_scatter(
        (
            jnp.dot(attn_out, differential_output_rows, preferred_element_type=jnp.float32)
            + jnp.dot(chain_out, linear_output_rows, preferred_element_type=jnp.float32)
        ).astype(jnp.bfloat16),
        "tp",
        scatter_dimension=0,
        tiled=True,
    )


def solution(mesh):
    placed = (
        P(("sp", "tp"), None),
        P(),
        P(None, "tp"),
        P(None, "tp"),
        P(None, "tp"),
        P(),
        P(),
        P("tp"),
        P(),
        P(None, "tp"),
        P(None, "tp"),
        P(None, "tp"),
        P(None, "tp"),
        P(),
        P(None, "tp"),
        P("tp"),
        P("sp", "tp"),
        P(),
        P("tp", None),
        P("tp", None),
    )
    return jax.shard_map(
        per_device, mesh=mesh, in_specs=placed, out_specs=P(("sp", "tp"), None), check_vma=False
    )
```

profile of v0, /device:TPU:25, one launch (start us, length us, event | category | flops | bytes accessed | tf_op | source)
XLA Modules:
  0.0 272.5 jit_solution(2683229393621899004)
XLA Ops:
  6.6 3.3 %constant_dynamic-update-slice_fusion.7 = bf16[2048,3104]{1,0:T(8,128)(2,1)} fusion(bf16[2048,512]{1,0:T(8,128)(2,1)} %param.30), kind=kLoop, calls=%fused_computation.130 | loop fusion | bytes 4194304
  10.5 2.6 all_gather.21
  13.2 3.2 %constant_dynamic-update-slice_fusion.6 = bf16[2048,3104]{1,0:T(8,128)(2,1)} fusion(bf16[2048,3104]{1,0:T(8,128)(2,1)} %constant_dynamic-update-slice_fusion.7, bf16[2048,512]{1,0:T(8,128)(2,1)} %param.31), kind=kLoop, calls=%fused_computation.129 | loop fusion | bytes 4194304
  16.4 1.5 constant_dynamic-update-slice_fusion.5
  18.0 1.1 constant_dynamic-update-slice_fusion.4
  19.0 1.1 constant_dynamic-update-slice_fusion.3
  20.1 1.6 constant_dynamic-update-slice_fusion.2
  21.7 1.5 constant_dynamic-update-slice_fusion.1
  24.1 8.3 %convolution_convert_fusion = bf16[128,3104]{0,1:T(8,128)(2,1)S(1)} fusion(bf16[128,2048]{1,0:T(8,128)(2,1)S(1)} %all_gather.21, bf16[2048,3104]{1,0:T(8,128)(2,1)} %constant_dynamic-update-slice_fusion), kind=kOutput, calls=%fused_computation.68 | convolution fusion | flops 1627787264 | bytes 14032896 | tf_op jit(solution)/shard_map/dot_general | solution.py:134
  35.6 1.1 reshape.228
  36.7 1.2 copy.125
  38.0 0.9 fusion.54
  38.9 1.1 div.64
  40.1 1.1 mul.296
  41.2 1.8 reshape.219
  43.0 0.9 broadcast_add_fusion
  43.9 10.5 %while.8 = (s32[]{:T(128)}, f32[4,64,128]{2,1,0:T(8,128)S(1)}, f32[4,64]{1,0:T(4,128)S(1)}, f32[2,64,4,128]{3,1,0,2:T(8,128)}, f32[2,64,4,64]{3,2,1,0:T(4,128)},...) while((s32[]{:T(128)}, f32[4,64,128]{2,1,0:T(8,128)S(1)}, ...), condition=%wide.region_17.18_spmd.clone, body=%wide.region_15.0_spmd.clone.sunk | while | flops 89412096 | bytes 2970753 | solution.py:259
  43.9 1.2 constant_dynamic-slice_fusion.3
  45.2 1.0 fusion.104
  47.1 0.9 fusion.105
  49.1 1.2 constant_dynamic-slice_fusion.3
  50.5 1.0 fusion.104
  52.3 0.9 fusion.105
  55.7 1.3 collective-permute-start
  57.0 2.3 collective-permute-done
  59.3 1.2 collective-permute-start.1
  62.5 1.1 copy.129
  63.6 26.2 %all-gather.2 = f32[16,4,64]{2,1,0:T(4,128)S(1)} all-gather(f32[1,4,64]{2,1,0:T(4,128)S(1)} %exponential_bitcast_fusion), channel_id=2, replica_groups=mesh['sp'=16,'tp'=2] {'sp'}, dimensions={0}, use_global_device_ids=true | all-gather | bytes 17408 | tf_op jit(solution)/shard_map/all_gather | solution.py:34
  89.8 6.5 %collective-permute-done.2 = bf16[64,512]{1,0:T(8,128)(2,1)S(1)} collective-permute-done((bf16[64,512]{1,0:T(8,128)(2,1)S(1)}, bf16[64,512]{1,0:T(8,128)(2,1)S(1)}, u32[]{:S(2)}, u32[]{:S(2)}) %collective-permute-start.2) | collective-permute-done | bytes 65568 | tf_op jit(solution)/shard_map/ppermute | solution.py:29
  96.3 3.4 %collective-permute-start.3 = (bf16[64,512]{1,0:T(8,128)(2,1)S(1)}, bf16[64,512]{1,0:T(8,128)(2,1)S(1)}, u32[]{:S(2)}, u32[]{:S(2)}) collective-permute-start(bf16[64,512]{1,0:T(8,128)(2,1)S(1)} %collective-permute-done.2), channel_id=1, source_target_pairs={{0,16},{16,0},{2,18},{18,2},{4,20},{20,4},{6,22},{22,6},{8,24},{24... | collective-permute-start | bytes 196616 | tf_op jit(solution)/shard_map/ppermute | solution.py:29
  99.7 60.6 %all-gather.9.cloned.1.call-done = bf16[2048,512]{0,1:T(8,128)(2,1)} async-done(((bf16[128,512]{0,1:T(8,128)(2,1)}), bf16[2048,512]{0,1:T(8,128)(2,1)}) %all-gather.9.cloned.1.call-update) | async-done | bytes 2097168 | tf_op jit(solution)/shard_map/all_gather | solution.py:174
  160.3 5.5 %conditional.3 = (f32[8,64]{1,0:T(8,128)S(1)}, f32[8,64,128]{2,1,0:T(8,128)S(1)}) conditional(s32[]{:T(128)} %convert_element_type.81, (f32[8,64]{1,0:T(8,128)S(1)}, f32[8,64,128]{2,1,0:T(8,128)S(1)}) %tuple.49, (s32[2048]{0:T(1024)S(1)}, s32[64]{0:T(128)S(1)}, bf16[64,512]{1,0:T(8,128)(2,1)S(1)}, bf16[2048,8,64]{0,2,1:T(8,128)(2,1)}, ...), branch_computations={%region_10.0_spmd, %region_11.0_spmd} | conditional | flops 412353536 | bytes 26839340 | solution.py:190
  160.7 2.6 fusion.9
  163.3 1.3 fusion.10
  165.8 5.2 %conditional.2 = ((f32[8,64]{1,0:T(8,128)S(1)}, f32[8,64,128]{2,1,0:T(8,128)S(1)})) conditional(s32[]{:T(128)} %convert_element_type.71, (f32[8,64]{1,0:T(8,128)S(1)}, f32[8,64,128]{2,1,0:T(8,128)S(1)}) %tuple.49, (s32[2048]{0:T(1024)S(1)}, s32[64]{0:T(128)S(1)}, bf16[128,8,64]{2,0,1:T(8,128)(2,1)S(1)}, bf16[2048,8,64]{0,2,1:T(8,128)(2,1)}, ...), branch_computations={%region_4.5_spmd, %region_5.8_spmd} | conditional | flops 412353536 | bytes 26773812 | solution.py:190
  166.0 2.6 fusion.2
  168.6 1.3 fusion.3
  172.6 48.8 %all-gather.11.cloned.1.call-done = f32[64,64,128]{2,1,0:T(8,128)} async-done(((f32[4,64,128]{2,1,0:T(8,128)}), f32[64,64,128]{2,1,0:T(8,128)}) %all-gather.11.cloned.1.call-update) | async-done | bytes 2097168 | tf_op jit(solution)/shard_map/all_gather | solution.py:34
  221.4 17.2 %while.9 = (s32[]{:T(128)}, f32[4,64,128]{2,1,0:T(8,128)S(1)}, s32[]{:T(128)}, f32[16,4,64]{2,1,0:T(4,128)S(1)}, f32[16,4,64,128]{3,2,1,0:T(8,128)}, /*index=5*/s32[]{:T(128)}, s32[]{:T(128)}) while((s32[]{:T(128)}, f32[4,64,128]{2,1,0:T(8,128)S(1)}, s32[]{:T(128)}, f32[16,4,64]{2,1,0:T(4,128)S(1)}, ...), condition=%wide.region_19.20_spmd.clone, body=%wide.region_18.19_spmd.clone.sunk | while | flops 131076 | bytes 396393 | solution.py:46
  221.4 1.0 fusion.107
  222.5 1.0 fusion.107
  223.6 1.0 fusion.107
  224.7 1.0 fusion.107
  225.8 1.0 fusion.107
  226.8 1.0 fusion.107
  227.9 1.0 fusion.107
  229.0 1.0 fusion.107
  230.1 1.0 fusion.107
  231.2 1.0 fusion.107
  232.2 1.0 fusion.107
  233.3 1.0 fusion.107
  234.4 1.0 fusion.107
  235.5 1.0 fusion.107
  236.6 1.0 fusion.107
  237.6 1.0 fusion.107
  238.7 1.7 multiply_reduce_fusion
  240.4 1.3 collective-permute-start.5
  241.7 1.9 collective-permute-done.5
  243.6 1.0 collective-permute-start.6
  244.7 2.0 collective-permute-done.6
  246.7 1.5 collective-permute-start.7
  248.7 2.0 collective-permute-done.7
  250.8 1.3 fusion.41
  252.0 14.0 %reduce-scatter.2.cloned.1.call-done = bf16[64,2048]{1,0:T(8,128)(2,1)} async-done(((bf16[128,2048]{1,0:T(8,128)(2,1)}), bf16[64,2048]{1,0:T(8,128)(2,1)}) %reduce-scatter.2.cloned.1.call-update) | async-done | bytes 262160 | tf_op jit(solution)/shard_map/reduce_scatter | solution.py:286
  (152 shorter events, 15.8 us)
Async XLA Ops:
  6.5 241.7 %copy-start = (bf16[512,2048]{1,0:T(8,128)(2,1)S(1)}, bf16[512,2048]{1,0:T(8,128)(2,1)}, u32[]{:S(2)}) copy-start(bf16[512,2048]{1,0:T(8,128)(2,1)} %param.47) | copy-start | bytes 6291460
  6.5 3.4 %copy-start.12 = (bf16[2048,32]{0,1:T(8,128)(2,1)S(1)}, bf16[2048,32]{0,1:T(8,128)(2,1)}, u32[]{:S(2)}) copy-start(bf16[2048,32]{0,1:T(8,128)(2,1)} %param.41) | copy-start | bytes 393220
  6.5 3.7 %copy-start.8 = (bf16[64,2048]{1,0:T(8,128)(2,1)S(1)}, bf16[64,2048]{1,0:T(8,128)(2,1)}, u32[]{:S(2)}) copy-start(bf16[64,2048]{1,0:T(8,128)(2,1)} %param.28) | copy-start | bytes 786436
  6.5 3.9 %copy-start.13 = (f32[2048]{0:T(1024)S(1)}, f32[2048]{0:T(1024)}, u32[]{:S(2)}) copy-start(f32[2048]{0:T(1024)} %param.29) | copy-start | bytes 24580
  6.5 93.1 %all-gather.7.cloned.1.call-start = ((), (), s32[]{:S(2)}) async-start(), calls=%async_computation.1 | async-start | bytes 2228224 | tf_op jit(solution)/shard_map/all_gather | solution.py:173
  10.2 6.2 %copy-start.4 = (bf16[2048,512]{1,0:T(8,128)(2,1)S(1)}, bf16[2048,512]{1,0:T(8,128)(2,1)}, u32[]{:S(2)}) copy-start(bf16[2048,512]{1,0:T(8,128)(2,1)} %param.32) | copy-start | bytes 6291460
  13.2 4.8 %copy-start.9 = (bf16[2048,256]{1,0:T(8,128)(2,1)S(1)}, bf16[2048,256]{1,0:T(8,128)(2,1)}, u32[]{:S(2)}) copy-start(bf16[2048,256]{1,0:T(8,128)(2,1)} %param.37) | copy-start | bytes 3145732
  16.4 2.6 copy-start.10
  16.4 3.7 %copy-start.5 = (bf16[2048,512]{1,0:T(8,128)(2,1)S(1)}, bf16[2048,512]{1,0:T(8,128)(2,1)}, u32[]{:S(2)}) copy-start(bf16[2048,512]{1,0:T(8,128)(2,1)} %param.39) | copy-start | bytes 6291460
  18.0 3.8 %copy-start.6 = (bf16[2048,512]{1,0:T(8,128)(2,1)S(1)}, bf16[2048,512]{1,0:T(8,128)(2,1)}, u32[]{:S(2)}) copy-start(bf16[2048,512]{1,0:T(8,128)(2,1)} %param.40) | copy-start | bytes 6291460
  24.1 8.4 %copy-start.16 = (f32[64]{0:T(128)S(1)}, f32[64]{0:T(128)}, u32[]{:S(2)}) copy-start(f32[64]{0:T(128)} %param.34) | copy-start | bytes 772
  24.1 13.8 %copy-start.20 = (bf16[32,256]{1,0:T(8,128)(2,1)S(1)}, bf16[32,256]{1,0:T(8,128)(2,1)}, u32[]{:S(2)}) copy-start(bf16[32,256]{1,0:T(8,128)(2,1)} %param.42) | copy-start | bytes 49156
  24.1 13.9 %copy-start.21 = (f32[256]{0:T(256)S(1)}, f32[256]{0:T(256)}, u32[]{:S(2)}) copy-start(f32[256]{0:T(256)} %param.43) | copy-start | bytes 3076
  32.4 7.6 %copy-start.14 = (f32[128,4]{0,1:T(4,128)S(1)}, f32[128,4]{0,1:T(4,128)}, u32[]{:S(2)}) copy-start(f32[128,4]{0,1:T(4,128)} %param.44) | copy-start | bytes 6148
  33.5 126.8 %all-gather.9.cloned.1.call-start = ((), (), s32[]{:S(2)}) async-start(), calls=%async_computation.2 | async-start | bytes 2228224 | tf_op jit(solution)/shard_map/all_gather | solution.py:174
  34.2 187.2 %all-gather.11.cloned.1.call-start = ((), (), s32[]{:S(2)}) async-start(), calls=%async_computation.4 | async-start | bytes 2228224 | tf_op jit(solution)/shard_map/all_gather | solution.py:34
  43.9 11.4 %copy-start.17 = (f32[64]{0:T(128)S(1)}, f32[64]{0:T(128)}, u32[]{:S(2)}) copy-start(f32[64]{0:T(128)} %param.33) | copy-start | bytes 772
  54.4 0.6 copy-start.3
  55.0 211.0 %reduce-scatter.2.cloned.1.call-start = ((), (), s32[]{:S(2)}) async-start(), calls=%async_computation.3 | async-start | bytes 786432 | tf_op jit(solution)/shard_map/reduce_scatter | solution.py:286
  55.7 3.6 %collective-permute-start = (bf16[64,512]{1,0:T(8,128)(2,1)S(1)}, bf16[64,512]{1,0:T(8,128)(2,1)S(1)}, u32[]{:S(2)}, u32[]{:S(2)}) collective-permute-start(bf16[64,512]{1,0:T(8,128)(2,1)S(1)} %reshape.212), channel_id=1, source_target_pairs={{0,2},{2,0},{4,6},{6,4},{8,10},{10,8},{12,14},{14,12},{16,18},{18,... | collective-permute-start | bytes 196616 | tf_op jit(solution)/shard_map/ppermute | solution.py:29
  59.3 30.5 %collective-permute-start.1 = (bf16[64,512]{1,0:T(8,128)(2,1)S(1)}, bf16[64,512]{1,0:T(8,128)(2,1)S(1)}, u32[]{:S(2)}, u32[]{:S(2)}) collective-permute-start(bf16[64,512]{1,0:T(8,128)(2,1)S(1)} %collective-permute-done), channel_id=1, source_target_pairs={{0,4},{4,0},{2,6},{6,2},{8,12},{12,8},{10,14},{14,10},{16,20},{20,... | collective-permute-start | bytes 196616 | tf_op jit(solution)/shard_map/ppermute | solution.py:29
  89.8 6.5 %collective-permute-start.2 = (bf16[64,512]{1,0:T(8,128)(2,1)S(1)}, bf16[64,512]{1,0:T(8,128)(2,1)S(1)}, u32[]{:S(2)}, u32[]{:S(2)}) collective-permute-start(bf16[64,512]{1,0:T(8,128)(2,1)S(1)} %collective-permute-done.1), channel_id=1, source_target_pairs={{0,8},{8,0},{2,10},{10,2},{4,12},{12,4},{6,14},{14,6},{16,24},{24,... | collective-permute-start | bytes 196616 | tf_op jit(solution)/shard_map/ppermute | solution.py:29
  96.3 63.9 %collective-permute-start.3 = (bf16[64,512]{1,0:T(8,128)(2,1)S(1)}, bf16[64,512]{1,0:T(8,128)(2,1)S(1)}, u32[]{:S(2)}, u32[]{:S(2)}) collective-permute-start(bf16[64,512]{1,0:T(8,128)(2,1)S(1)} %collective-permute-done.2), channel_id=1, source_target_pairs={{0,16},{16,0},{2,18},{18,2},{4,20},{20,4},{6,22},{22,6},{8,24},{24... | collective-permute-start | bytes 196616 | tf_op jit(solution)/shard_map/ppermute | solution.py:29
  163.3 1.6 copy-start.1
  165.8 5.7 %copy-start.15 = (f32[4]{0:T(128)S(1)}, f32[4]{0:T(128)}, u32[]{:S(2)}) copy-start(f32[4]{0:T(128)} %param.35) | copy-start | bytes 52
  165.8 6.1 %copy-start.18 = (f32[128]{0:T(128)S(1)}, f32[128]{0:T(128)}, u32[]{:S(2)}) copy-start(f32[128]{0:T(128)} %param.36) | copy-start | bytes 1540
  168.6 1.6 copy-start.2
  171.1 73.6 %copy-start.11 = (f32[128,512]{0,1:T(8,128)S(1)}, f32[128,512]{0,1:T(8,128)}, u32[]{:S(2)}) copy-start(f32[128,512]{0,1:T(8,128)} %get-tuple-element.532) | copy-start | bytes 786436
  171.1 73.5 %copy-start.19 = (f32[128]{0:T(128)S(1)}, f32[128]{0:T(128)}, u32[]{:S(2)}) copy-start(f32[128]{0:T(128)} %param.45) | copy-start | bytes 1540
  172.3 68.1 %collective-permute-start.4 = (bf16[64,512]{1,0:T(8,128)(2,1)S(1)}, bf16[64,512]{1,0:T(8,128)(2,1)S(1)}, u32[]{:S(2)}, u32[]{:S(2)}) collective-permute-start(bf16[64,512]{1,0:T(8,128)(2,1)S(1)} %bitcast.194), channel_id=1, source_target_pairs={{0,2},{2,0},{4,6},{6,4},{8,10},{10,8},{12,14},{14,12},{16,18},{18,... | collective-permute-start | bytes 196616 | tf_op jit(solution)/shard_map/ppermute | solution.py:29
  238.7 12.1 %copy-start.7 = (bf16[512,2048]{1,0:T(8,128)(2,1)S(1)}, bf16[512,2048]{1,0:T(8,128)(2,1)}, u32[]{:S(2)}) copy-start(bf16[512,2048]{1,0:T(8,128)(2,1)} %param.46) | copy-start | bytes 6291460
  240.4 3.2 %collective-permute-start.5 = (bf16[64,512]{1,0:T(8,128)(2,1)S(1)}, bf16[64,512]{1,0:T(8,128)(2,1)S(1)}, u32[]{:S(2)}, u32[]{:S(2)}) collective-permute-start(bf16[64,512]{1,0:T(8,128)(2,1)S(1)} %collective-permute-done.4), channel_id=1, source_target_pairs={{0,4},{4,0},{2,6},{6,2},{8,12},{12,8},{10,14},{14,10},{16,20},{20,... | collective-permute-start | bytes 196616 | tf_op jit(solution)/shard_map/ppermute | solution.py:29
  243.6 3.1 %collective-permute-start.6 = (bf16[64,512]{1,0:T(8,128)(2,1)S(1)}, bf16[64,512]{1,0:T(8,128)(2,1)S(1)}, u32[]{:S(2)}, u32[]{:S(2)}) collective-permute-start(bf16[64,512]{1,0:T(8,128)(2,1)S(1)} %collective-permute-done.5), channel_id=1, source_target_pairs={{0,8},{8,0},{2,10},{10,2},{4,12},{12,4},{6,14},{14,6},{16,24},{24,... | collective-permute-start | bytes 196616 | tf_op jit(solution)/shard_map/ppermute | solution.py:29
  246.7 4.0 %collective-permute-start.7 = (bf16[64,512]{1,0:T(8,128)(2,1)S(1)}, bf16[64,512]{1,0:T(8,128)(2,1)S(1)}, u32[]{:S(2)}, u32[]{:S(2)}) collective-permute-start(bf16[64,512]{1,0:T(8,128)(2,1)S(1)} %collective-permute-done.6), channel_id=1, source_target_pairs={{0,16},{16,0},{2,18},{18,2},{4,20},{20,4},{6,22},{22,6},{8,24},{24... | collective-permute-start | bytes 196616 | tf_op jit(solution)/shard_map/ppermute | solution.py:29
Sparse Core Ops, SparseCore 0:
  33.6 62.0 all-gather.6
  98.4 61.7 all-gather.8
  163.0 58.3 all-gather.10
  252.2 13.7 reduce-scatter.1
where the time goes:
time: 274 us; the launch traced here: 273 us
  waiting for transfers between devices  138 us (50%)
  other arithmetic  29.7 us (11%)
  blocking collectives  28.8 us (11%)
  local copies, waits for them, and re-layouts  27 us (10%)
  matrix products  23.1 us (8%)
  between operations  14.8 us (5%)
  starting transfers between devices  10.1 us (4%)
    all_gather x1, waiting for transfers between devices, per_device(): value_rows = lax.all_gather(value_flat, 'sp', axis=0, tiled=True)  60.6 us
    all_gather x1, waiting for transfers between devices, prefix(): everything = jax.tree.map(lambda part: lax.all_gather(part, axis), shard)  48.8 us
    all_gather x1, blocking collectives, prefix(): everything = jax.tree.map(lambda part: lax.all_gather(part, axis), shard)  26.2 us
    select_n x16, other arithmetic, turn(): return jax.tree.map(lambda a, b: jnp.where(reached, a, b), new, before)  16.6 us
    unnamed x52, local copies, waits for them, and re-layouts  15.6 us
    ppermute x8, waiting for transfers between devices, partner(): return lax.ppermute(block, axis, route)  14.7 us
    reduce_scatter x1, waiting for transfers between devices, per_device(): lax.psum_scatter((jnp.dot(attn_out, differential_output_rows, preferred_e...  14 us
    ppermute x8, starting transfers between devices, partner(): return lax.ppermute(block, axis, route)  9.9 us
  transfers between devices with their start and end apart: 12, of which 8 were waited for; matrix products, arithmetic and copies ran while one was open for 19% of the time, Pallas kernels for 0%

commit v1 on v0

v1 whole, which is shorter than its diff:
```python
import functools

import jax
import jax.numpy as jnp
import numpy as np
from jax import lax
from jax.experimental import pallas as pl
from jax.experimental.pallas import tpu as pltpu
from jax.sharding import PartitionSpec as P

HEAD = 64
VDIM = 128
RECURRENT_DIM = 64
LANES = 128
RMS_EPS = 1e-06
OUT_SCALE = 0.8
MESH = pl.DeviceIdType.MESH
F32 = jnp.float32
BF16 = jnp.bfloat16


def dot(a, b):
    return jnp.dot(a, b, preferred_element_type=F32)


def dot_t(a, b):
    return lax.dot_general(a, b, (((1,), (1,)), ((), ())), preferred_element_type=F32)


def decay_tables(rows):
    levels = rows.bit_length() - 1
    t = np.arange(rows)[:, None]
    r = np.arange(rows)[None, :]
    parts = []
    for level in range(levels):
        h = 1 << level
        mid = (t // (2 * h)) * 2 * h + h - 1
        upper = (t // h) % 2 == 1
        parts.append(np.where(upper, (r > mid) & (r <= t), (r > t) & (r <= mid)))
    parts.append(r <= t)
    parts.append(r > t)
    pair_level = np.full((rows, rows), -1, np.int32)
    for level in range(levels):
        pair_level[((t ^ r) >> level == 1) & (t > r)] = level
    pair_level[t == r] = levels
    return np.concatenate(parts, 0).astype(np.float32), pair_level, levels


def body(
    cfg,
    tokens, gain, wq, wk, wv, wlq, wlk, wlv, wlg, wdown, up, bias, extra, qgain, kgain, lam,
    dgain, lgain, wo1, wo2, table, pair_level,
    out,
    xbuf, xn, wbuf, wl, ebuf, proj, plin, logs, kv, q2, acc, peak, total, wo, qd, inner, states,
    pre, pref_in, pref_out, obuf, mix, terms, got,
    w_sem, xs_in, xs_tp, x_recv, es, er, kv_send, kv_recv, st_send, st_recv, a_send, a_recv,
    c_send, c_recv, t_send, t_recv,
):
    G, N, T, r, R, S, D, LW, levels = cfg
    sp = lax.axis_index("sp")
    t = lax.axis_index("tp")
    o = lax.div(sp, G)
    i = lax.rem(sp, G)
    wide = LW == LANES
    pairs = LANES // RECURRENT_DIM

    col = pl.multiple_of(i * LANES, LANES)
    lcol = pl.multiple_of(lax.div(i, pairs) * LANES, LANES) if wide else 0
    loads = []
    for n, w in enumerate((wq, wk, wv, wlv, wlg)):
        loads.append(
            pltpu.make_async_copy(
                w.at[:, pl.ds(col, LANES)], wbuf.at[:, pl.ds(n * LANES, LANES)], w_sem.at[n]
            )
        )
    for n, w in enumerate((wlq, wlk)):
        src = w.at[:, pl.ds(lcol, LW)] if wide else w
        dst = wbuf.at[:, pl.ds((5 + n) * LANES, LANES)] if wide else wl.at[n]
        loads.append(pltpu.make_async_copy(src, dst, w_sem.at[5 + n]))
    for copy in loads:
        copy.start()
    wo_loads = [
        pltpu.make_async_copy(w, wo.at[n], w_sem.at[7 + n]) for n, w in enumerate((wo1, wo2))
    ]
    for copy in wo_loads:
        copy.start()

    def peer(d):
        return o * G + lax.rem(i + d, G)

    def source(d):
        return lax.rem(i - d + G, G)

    def tpeer(k):
        return lax.rem(t + k, T)

    barrier = pltpu.get_barrier_semaphore()
    for d in range(G):
        for k in range(T):
            if d or k:
                pl.semaphore_signal(
                    barrier, inc=1, device_id=(peer(d), tpeer(k)), device_id_type=MESH
                )

    @pl.when(o > 0)
    def _():
        pl.semaphore_signal(barrier, inc=1, device_id=(sp - G, t), device_id_type=MESH)

    @pl.when(o < N - 1)
    def _():
        pl.semaphore_signal(barrier, inc=1, device_id=(sp + G, t), device_id_type=MESH)

    inside = (o > 0) & (o < N - 1)

    @pl.when(inside)
    def _():
        pl.semaphore_wait(barrier, G * T + 1)

    @pl.when(jnp.logical_not(inside))
    def _():
        pl.semaphore_wait(barrier, G * T if N > 1 else G * T - 1)

    def remote(src, dst, ss, rs, where):
        return pltpu.make_async_remote_copy(
            src_ref=src, dst_ref=dst, send_sem=ss, recv_sem=rs, device_id=where,
            device_id_type=MESH,
        )

    own = i * T + t
    sends = []
    for k in range(1, T):
        sends.append(
            remote(tokens, xbuf.at[own], xs_tp.at[k], x_recv.at[own], (sp, tpeer(k)))
        )
    for d in range(1, G):
        sends.append(remote(tokens, xbuf.at[own], xs_in.at[d], x_recv.at[own], (peer(d), t)))
    for d in range(1, G):
        sends.append(remote(extra, ebuf.at[i], es.at[d], er.at[i], (peer(d), t)))
    for copy in sends:
        copy.start()
    xbuf[own] = tokens[...]
    ebuf[i] = extra[...]

    def arrival(slot):
        remote(
            tokens, xbuf.at[slot], xs_in.at[0], x_recv.at[slot], (peer(1) if G > 1 else sp, tpeer(1))
        ).wait_recv()

    def forward(d):
        j = source(d)
        slot = j * T + t
        arrival(slot)
        for k in range(1, T):
            copy = remote(
                xbuf.at[slot], xbuf.at[slot], xs_tp.at[d * T + k], x_recv.at[slot], (sp, tpeer(k))
            )
            copy.start()
            sends.append(copy)

    lane = lax.broadcasted_iota(jnp.int32, (1, LANES), 1)
    low_half = lane < HEAD

    def map_norm(values, map_gain):
        sq = values * values
        first = jnp.sum(jnp.where(low_half, sq, 0.0), axis=-1, keepdims=True)
        second = jnp.sum(jnp.where(low_half, 0.0, sq), axis=-1, keepdims=True)
        scale = jnp.where(
            low_half,
            lax.rsqrt(first * (1.0 / HEAD) + RMS_EPS),
            lax.rsqrt(second * (1.0 / HEAD) + RMS_EPS),
        )
        return values * scale * map_gain

    def project(d):
        j = source(d)
        for k in range(1, T):
            arrival(j * T + tpeer(k))
        if d > 0:
            remote(extra, ebuf.at[j], es.at[0], er.at[j], (peer(1), t)).wait_recv()
        for c in range(T):
            x = xbuf[j * T + c].astype(F32)
            ms = jnp.mean(x * x, axis=-1, keepdims=True)
            xn[pl.ds(c * r, r), :] = (x * lax.rsqrt(ms + RMS_EPS) * gain[...]).astype(BF16)
        if d == 0:
            for copy in loads:
                copy.wait()
        x = xn[...]
        rows = pl.ds(pl.multiple_of(j * R, R), R)
        proj_block = dot(x, wbuf[...]).astype(BF16)
        qn = map_norm(proj_block[:, 0:LANES].astype(F32), qgain[...]).astype(BF16) * HEAD ** (-0.5)
        qn = qn.astype(BF16)
        zero = jnp.zeros_like(qn)
        q2[0, rows, :] = jnp.where(low_half, qn, zero)
        q2[1, rows, :] = jnp.where(low_half, zero, qn)
        kn = map_norm(proj_block[:, LANES : 2 * LANES].astype(F32), kgain[...]).astype(BF16)
        kv[o, rows, 0:LANES] = kn
        kv[o, rows, LANES : 2 * LANES] = proj_block[:, 2 * LANES : 3 * LANES]
        proj[rows, :] = proj_block[:, 3 * LANES : 5 * LANES]
        if wide:
            mine = lax.div(lane, RECURRENT_DIM) == lax.rem(i, pairs)
            for n in range(2):
                part = proj_block[:, (5 + n) * LANES : (6 + n) * LANES]
                plin[n, rows, :] = jnp.where(mine, part, jnp.zeros_like(part))
        else:
            for n in range(2):
                plin[n, rows, :] = dot(x, wl[n]).astype(BF16)
        low = dot(x, wdown[...]).astype(BF16)
        lsl = pl.ds(lcol, LW)
        pre_act = dot(low, up[:, lsl]) + bias[:, lsl]
        log_sig = jnp.minimum(pre_act, 0.0) - jnp.log1p(jnp.exp(-jnp.abs(pre_act)))
        turned = ebuf[j].T
        head_lane = lax.broadcasted_iota(jnp.int32, (1, turned.shape[1]), 1)
        add = jnp.sum(jnp.where(head_lane == i, turned, 0.0), axis=1, keepdims=True)
        logs[rows, :] = log_sig * (1.0 / 16.0) + add

    if G > 1:
        forward(1)
    for d in range(G):
        if 0 < d and d + 1 < G:
            forward(d + 1)
        elif d == 0 and G > 1:
            pass
        project(d)

    def kv_copy(slot):
        return remote(
            kv.at[slot], kv.at[slot], kv_send.at[slot], kv_recv.at[slot], (sp + G, t)
        )

    @pl.when(o < N - 1)
    def _():
        kv_copy(o).start()

    level_of = pair_level[...]
    states[...] = jnp.zeros_like(states)
    pre[...] = jnp.zeros_like(pre)

    def chain_block(b, _):
        rows = pl.ds(pl.multiple_of(b * R, R), R)
        la = logs[rows, :]
        hi = la.astype(BF16)
        lo = (la - hi.astype(F32)).astype(BF16)
        q = plin[0, rows, :].astype(F32) * RECURRENT_DIM ** (-0.5)
        k = plin[1, rows, :].astype(F32)
        v = proj[rows, 0:LANES]
        sums = dot(table[...], hi) + dot(table[...], lo)
        scores = jnp.where(level_of == levels, dot_t(q.astype(BF16), k.astype(BF16)), 0.0)
        for level in range(levels):
            e = jnp.exp(sums[level * R : (level + 1) * R])
            part = dot_t((q * e).astype(BF16), (k * e).astype(BF16))
            scores = scores + jnp.where(level_of == level, part, 0.0)
        inner[rows, :] = dot(scores.astype(BF16), v)
        cum = sums[levels * R : (levels + 1) * R]
        suffix = sums[(levels + 1) * R : (levels + 2) * R]
        qd[rows, :] = (q * jnp.exp(cum)).astype(BF16)
        k_end = (k * jnp.exp(suffix)).astype(BF16)
        last = cum[R - 1 : R, :]
        vt = v.astype(F32).T.astype(BF16)
        states[b + 1] = states[b] * jnp.exp(last) + dot(vt, k_end)
        pre[b + 1] = pre[b] + last
        return 0

    lax.fori_loop(0, G, chain_block, 0)

    def prefix_copy():
        return remote(
            pref_out.at[...], pref_in.at[...], st_send.at[0], st_recv.at[0], (sp + G, t)
        )

    TQ = min(2 * LANES, S)

    def attend(slot, first):
        k = kv.at[slot]

        def tile(j, _):
            m = lax.div(j, S // TQ)
            start = pl.multiple_of(lax.rem(j, S // TQ) * TQ, TQ)
            rows = pl.ds(start, TQ)
            s = dot_t(q2[m, rows, :], k[:, 0:LANES])
            if first:
                u = lax.broadcasted_iota(jnp.int32, (TQ, S), 1)
                tt = lax.broadcasted_iota(jnp.int32, (TQ, S), 0) + start
                s = jnp.where(u <= tt, s, -1e30)
                new = jnp.max(s, axis=-1, keepdims=True)
                p = jnp.exp(s - new)
                total[m, rows, :] = jnp.broadcast_to(
                    jnp.sum(p, axis=-1, keepdims=True), (TQ, LANES)
                )
                acc[m, rows, :] = dot(p.astype(BF16), k[:, LANES : 2 * LANES])
                peak[m, rows, :] = jnp.broadcast_to(new, (TQ, LANES))
            else:
                old = peak[m, rows, :]
                new = jnp.maximum(old, jnp.max(s, axis=-1, keepdims=True))
                p = jnp.exp(s - new[:, 0:1])
                factor = jnp.exp(old - new)
                total[m, rows, :] = total[m, rows, :] * factor + jnp.sum(
                    p, axis=-1, keepdims=True
                )
                acc[m, rows, :] = acc[m, rows, :] * factor + dot(
                    p.astype(BF16), k[:, LANES : 2 * LANES]
                )
                peak[m, rows, :] = new
            return 0

        lax.fori_loop(0, 2 * S // TQ, tile, 0)

    attend(o, True)

    def take(slot):
        kv_copy(slot).wait_recv()

        @pl.when(o < N - 1)
        def _():
            kv_copy(slot).start()

    @pl.when(o > 0)
    def _():
        take(o - 1)
        prefix_copy().wait_recv()

    @pl.when(o == 0)
    def _():
        pref_in[...] = jnp.zeros_like(pref_in)

    carried = pref_in[...]

    @pl.when(o < N - 1)
    def _():
        pref_out[...] = carried * jnp.exp(pre[G]) + states[G]
        prefix_copy().start()

    def chain_finish(b, _):
        rows = pl.ds(pl.multiple_of(b * R, R), R)
        state = (states[b] + pref_in[...] * jnp.exp(pre[b])).astype(BF16)
        full = inner[rows, :] + dot_t(qd[rows, :], state)
        gate = proj[rows, LANES : 2 * LANES].astype(F32)
        ms = jnp.mean(full * full, axis=-1, keepdims=True)
        gate = gate / (1.0 + jnp.exp(-gate))
        obuf[1, b] = (full * lax.rsqrt(ms + RMS_EPS) * lgain[...] * gate).astype(BF16)
        return 0

    lax.fori_loop(0, G, chain_finish, 0)

    def give(n, ss, rs):
        copies = []
        for d in range(1, G):
            j = lax.rem(i + d, G)
            copies.append(
                remote(obuf.at[n, j], mix.at[n, i], ss.at[d], rs.at[i], (peer(d), t))
            )
        for copy in copies:
            copy.start()
        mix[n, i] = obuf[n, i]
        return copies

    def collect(n, ss, rs):
        for d in range(1, G):
            j = source(d)
            remote(obuf.at[n, j], mix.at[n, j], ss.at[0], rs.at[j], (peer(1), t)).wait_recv()

    sends += give(1, c_send, c_recv)

    def earlier(s, _):
        slot = o - s

        @pl.when(s > 1)
        def _():
            take(slot)

        attend(slot, False)
        return 0

    lax.fori_loop(1, o + 1, earlier, 0)

    weight = lam[i]

    def attn_finish(b, _):
        rows = pl.ds(pl.multiple_of(b * R, R), R)
        diff = acc[0, rows, :] / total[0, rows, :] - weight * (
            acc[1, rows, :] / total[1, rows, :]
        )
        ms = jnp.mean(diff * diff, axis=-1, keepdims=True)
        obuf[0, b] = (diff * lax.rsqrt(ms + RMS_EPS) * dgain[...] * OUT_SCALE).astype(BF16)
        return 0

    lax.fori_loop(0, G, attn_finish, 0)
    sends += give(0, a_send, a_recv)
    for copy in wo_loads:
        copy.wait()
    collect(1, c_send, c_recv)
    chain_mix = jnp.concatenate([mix[1, j] for j in range(G)], axis=1)
    chain_part = dot(chain_mix, wo[1])
    collect(0, a_send, a_recv)
    attn_mix = jnp.concatenate([mix[0, j] for j in range(G)], axis=1)
    term = (dot(attn_mix, wo[0]) + chain_part).astype(BF16)
    for c in range(T):
        terms[c] = term[c * r : (c + 1) * r]
    for k in range(1, T):
        copy = remote(terms.at[tpeer(k)], got.at[t], t_send.at[k], t_recv.at[t], (sp, tpeer(k)))
        copy.start()
        sends.append(copy)
    summed = terms[t].astype(F32)
    for k in range(1, T):
        c = tpeer(k)
        remote(terms.at[c], got.at[c], t_send.at[0], t_recv.at[c], (sp, c)).wait_recv()
        summed = summed + got[c].astype(F32)
    out[...] = summed.astype(BF16)

    for copy in sends:
        copy.wait_send()

    @pl.when(o < N - 1)
    def _():
        prefix_copy().wait_send()

        def drain(s, _):
            kv_copy(s).wait_send()
            return 0

        lax.fori_loop(0, o + 1, drain, 0)


def per_device(
    tokens, input_norm_gain, differential_query, differential_key, differential_value,
    query_norm_gain, key_norm_gain, second_map_weight, differential_norm_gain, linear_query,
    linear_key, linear_value, linear_output_gate, forget_down_factor, forget_up_factor,
    forget_bias, extra_shrinkage_exponent, linear_norm_gain, differential_output_rows,
    linear_output_rows,
):
    sp_size, T = lax.axis_size("sp"), lax.axis_size("tp")
    G = second_map_weight.shape[0]
    r, D = tokens.shape
    R = r * T
    N = sp_size // G
    S = G * R
    LW = min(LANES, G * RECURRENT_DIM)
    table, pair_level, levels = decay_tables(R)
    cfg = (G, N, T, r, R, S, D, LW, levels)
    row = lambda a: a.reshape(1, -1)
    extra = jnp.pad(extra_shrinkage_exponent.T, ((0, -G % 8), (0, 0)))
    vmem = pl.BlockSpec(memory_space=pltpu.VMEM)
    smem = pl.BlockSpec(memory_space=pltpu.SMEM)
    anys = pl.BlockSpec(memory_space=pl.ANY)
    wide = LW == LANES
    dma = pltpu.SemaphoreType.DMA
    return pl.pallas_call(
        functools.partial(body, cfg),
        out_shape=jax.ShapeDtypeStruct((r, D), BF16),
        in_specs=[vmem] * 2 + [anys] * 7 + [vmem] * 6 + [smem] + [vmem] * 2 + [anys] * 2 + [vmem] * 2,
        out_specs=vmem,
        scratch_shapes=[
            pltpu.VMEM((G * T, r, D), BF16),
            pltpu.VMEM((R, D), BF16),
            pltpu.VMEM((D, (7 if wide else 5) * LANES), BF16),
            pltpu.VMEM((2, 16, LANES) if wide else (2, D, LW), BF16),
            pltpu.VMEM((G,) + extra.shape, F32),
            pltpu.VMEM((S, 2 * LANES), BF16),
            pltpu.VMEM((2, S, LW), BF16),
            pltpu.VMEM((S, LW), F32),
            pltpu.VMEM((N, S, 2 * LANES), BF16),
            pltpu.VMEM((2, S, LANES), BF16),
            pltpu.VMEM((2, S, LANES), F32),
            pltpu.VMEM((2, S, LANES), F32),
            pltpu.VMEM((2, S, LANES), F32),
            pltpu.VMEM((2,) + differential_output_rows.shape, BF16),
            pltpu.VMEM((S, LW), BF16),
            pltpu.VMEM((S, LANES), F32),
            pltpu.VMEM((G + 1, VDIM, LW), F32),
            pltpu.VMEM((G + 1, 1, LW), F32),
            pltpu.VMEM((VDIM, LW), F32),
            pltpu.VMEM((VDIM, LW), F32),
            pltpu.VMEM((2, G, R, LANES), BF16),
            pltpu.VMEM((2, G, R, LANES), BF16),
            pltpu.VMEM((T, r, D), BF16),
            pltpu.VMEM((T, r, D), BF16),
            dma((9,)),
            dma((G,)),
            dma((G * T,)),
            dma((G * T,)),
            dma((G,)),
            dma((G,)),
            dma((N,)),
            dma((N,)),
            dma((1,)),
            dma((1,)),
            dma((G,)),
            dma((G,)),
            dma((G,)),
            dma((G,)),
            dma((T,)),
            dma((T,)),
        ],
        compiler_params=pltpu.CompilerParams(
            collective_id=0, has_side_effects=True, vmem_limit_bytes=60 * 1024 * 1024
        ),
        name="layer",
    )(
        tokens, row(input_norm_gain), differential_query, differential_key, differential_value,
        linear_query, linear_key, linear_value, linear_output_gate, forget_down_factor,
        forget_up_factor, row(forget_bias), extra,
        row(jnp.tile(query_norm_gain, 2)), row(jnp.tile(key_norm_gain, 2)), second_map_weight,
        row(differential_norm_gain), row(linear_norm_gain), differential_output_rows,
        linear_output_rows, jnp.asarray(table, BF16), jnp.asarray(pair_level),
    )


def solution(mesh):
    placed = (
        P(("sp", "tp"), None),
        P(),
        P(None, "tp"),
        P(None, "tp"),
        P(None, "tp"),
        P(),
        P(),
        P("tp"),
        P(),
        P(None, "tp"),
        P(None, "tp"),
        P(None, "tp"),
        P(None, "tp"),
        P(),
        P(None, "tp"),
        P("tp"),
        P("sp", "tp"),
        P(),
        P("tp", None),
        P("tp", None),
    )
    return jax.shard_map(
        per_device, mesh=mesh, in_specs=placed, out_specs=P(("sp", "tp"), None), check_vma=False
    )
```

time: 274 us -> 62.4 us (0.23)
  waiting for transfers between devices: 138 us -> 0 us
  Pallas kernels: 0 us -> 54.8 us
  other arithmetic: 29.7 us -> 0 us
  blocking collectives: 28.8 us -> 0 us
  matrix products: 23.1 us -> 0 us
  local copies, waits for them, and re-layouts: 27 us -> 7.38 us
  between operations: 14.8 us -> 0.01 us
  starting transfers between devices: 10.1 us -> 0 us
    all_gather x3 -> x0, waiting for transfers between devices: 109 us -> none  [the longest x1 60.6 us: per_device(): value_rows = lax.all_gather(value_flat, 'sp', axis=0, tiled=True)]
    pallas_call x0 -> x1, Pallas kernels: none -> 54.8 us  [per_device(): pl.pallas_call(functools.partial(body, cfg), out_shape=jax.ShapeDtypeStru...]
    all_gather x2 -> x0, blocking collectives: 28.8 us -> none  [the longest x1 26.2 us: prefix(): everything = jax.tree.map(lambda part: lax.all_gather(part, axis), shard)]
    dot_general x17 -> x0, matrix products: 23.1 us -> none  [the longest x1 8.26 us: per_device(): jnp.dot(lax.all_gather(normed, 'tp', axis=0, tiled=True), packed, preferr...]
    select_n x16 -> x0, other arithmetic: 16.6 us -> none  [turn(): return jax.tree.map(lambda a, b: jnp.where(reached, a, b), new, before)]
    ppermute x8 -> x0, waiting for transfers between devices: 14.7 us -> none  [partner(): return lax.ppermute(block, axis, route)]
    reduce_scatter x1 -> x0, waiting for transfers between devices: 14 us -> none  [per_device(): lax.psum_scatter((jnp.dot(attn_out, differential_output_rows, preferred_e...]
    unnamed x52 -> x2, local copies, waits for them, and re-layouts: 15.6 us -> 3.57 us
  transfers between devices with their start and end apart: 12 -> 0, of which waited for: 8 -> 0; matrix products, arithmetic and copies ran while one was open for 19% -> 0% of each run, Pallas kernels for 0% -> 0%
where the time goes in v1:
time: 62.4 us; the launch traced here: 62.2 us
  Pallas kernels  54.8 us (88%)
  local copies, waits for them, and re-layouts  7.38 us (12%)
    pallas_call x1, Pallas kernels, per_device(): pl.pallas_call(functools.partial(body, cfg), out_shape=jax.ShapeDtypeStru...  54.8 us
    unnamed x2, local copies, waits for them, and re-layouts  3.57 us
    pad x1, local copies, waits for them, and re-layouts, per_device(): extra = jnp.pad(extra_shrinkage_exponent.T, ((0, -G % 8), (0, 0)))  1.28 us

profile of v1, /device:TPU:25, one launch (start us, length us, event | category | flops | bytes accessed | tf_op | source)
XLA Modules:
  0.0 62.2 jit_solution(17675384453268722274)
XLA Ops:
  0.0 0.7 %tile.4 = f32[2,64]{1,0:T(2,128)S(1)} broadcast(f32[64]{0:T(128)} %param.27), dimensions={1} | broadcast | bytes 768 | tf_op jit(solution)/shard_map/tile | solution.py:501
  0.7 0.7 %reshape_tile.6.qgain = f32[1,128]{1,0:T(1,128)} reshape(f32[2,64]{1,0:T(2,128)S(1)} %tile.4) | data formatting | bytes 1024 | tf_op jit(solution)/shard_map/reshape;tile | solution.py:439
  1.3 0.7 %tile.5 = f32[2,64]{1,0:T(2,128)S(1)} broadcast(f32[64]{0:T(128)} %param.28), dimensions={1} | broadcast | bytes 768 | tf_op jit(solution)/shard_map/tile | solution.py:501
  2.0 0.6 reshape_tile.7.kgain
  2.5 1.3 %pad.4.extra = f32[8,128]{1,0:T(8,128)} pad(f32[4,128]{1,0:T(4,128)} %bitcast.6, f32[]{:T(128)} %constant.6.clone.1), padding=0_4x0_0 | pad | bytes 6148 | tf_op jit(solution)/shard_map/jit(_pad)/pad | solution.py:440
  3.8 1.9 %copy.23.wdown = bf16[2048,32]{1,0:T(8,128)(2,1)} copy(bf16[2048,32]{0,1:T(8,128)(2,1)} %param.35) | data formatting | bytes 262144 | tf_op args[13]
  5.7 54.8 %layer.1 = bf16[64,2048]{1,0:T(8,128)(2,1)} custom-call(bf16[64,2048]{1,0:T(8,128)(2,1)} %tokens.1, f32[1,2048]{1,0:T(1,128)} %bitcast.5, bf16[2048,512]{1,0:T(8,128)(2,1)} %wq.1, bf16[2048,512]{1,0:T(8,128)(2,1)} %wk.1, bf16[2048,512]{1,0:T(8,128)(2,1)} %wv.1, bf16[2048,256]{1,0:T(8,128)(2,1)} %wlq.1, bf16[2048,256]{1,0:T(8,128)(2,1)} %wlk.1, ...), custom_call_target="tpu_custom_call" | custom-call | tf_op jit(solution)/shard_map/layer/pallas_call | solution.py:446
  60.5 1.7 %copy.25 = bf16[64,2048]{1,0:T(8,128)(2,1)} copy(bf16[64,2048]{1,0:T(8,128)(2,1)} %layer.1) | data formatting | bytes 524288

commit v2 on v1

--- a/solution.py
+++ b/solution.py
@@ -82,8 +82,6 @@
     wo_loads = [
         pltpu.make_async_copy(w, wo.at[n], w_sem.at[7 + n]) for n, w in enumerate((wo1, wo2))
     ]
-    for copy in wo_loads:
-        copy.start()
 
     def peer(d):
         return o * G + lax.rem(i + d, G)
@@ -160,6 +158,9 @@
     lane = lax.broadcasted_iota(jnp.int32, (1, LANES), 1)
     low_half = lane < HEAD
 
+    qg = jnp.concatenate([qgain[...], qgain[...]], axis=1)
+    kg = jnp.concatenate([kgain[...], kgain[...]], axis=1)
+
     def map_norm(values, map_gain):
         sq = values * values
         first = jnp.sum(jnp.where(low_half, sq, 0.0), axis=-1, keepdims=True)
@@ -184,15 +185,17 @@
         if d == 0:
             for copy in loads:
                 copy.wait()
+            for copy in wo_loads:
+                copy.start()
         x = xn[...]
         rows = pl.ds(pl.multiple_of(j * R, R), R)
         proj_block = dot(x, wbuf[...]).astype(BF16)
-        qn = map_norm(proj_block[:, 0:LANES].astype(F32), qgain[...]).astype(BF16) * HEAD ** (-0.5)
+        qn = map_norm(proj_block[:, 0:LANES].astype(F32), qg).astype(BF16) * HEAD ** (-0.5)
         qn = qn.astype(BF16)
         zero = jnp.zeros_like(qn)
         q2[0, rows, :] = jnp.where(low_half, qn, zero)
         q2[1, rows, :] = jnp.where(low_half, zero, qn)
-        kn = map_norm(proj_block[:, LANES : 2 * LANES].astype(F32), kgain[...]).astype(BF16)
+        kn = map_norm(proj_block[:, LANES : 2 * LANES].astype(F32), kg).astype(BF16)
         kv[o, rows, 0:LANES] = kn
         kv[o, rows, LANES : 2 * LANES] = proj_block[:, 2 * LANES : 3 * LANES]
         proj[rows, :] = proj_block[:, 3 * LANES : 5 * LANES]
@@ -204,32 +207,45 @@
         else:
             for n in range(2):
                 plin[n, rows, :] = dot(x, wl[n]).astype(BF16)
-        low = dot(x, wdown[...]).astype(BF16)
+        low = dot_t(x, wdown[...]).astype(BF16)
         lsl = pl.ds(lcol, LW)
         pre_act = dot(low, up[:, lsl]) + bias[:, lsl]
         log_sig = jnp.minimum(pre_act, 0.0) - jnp.log1p(jnp.exp(-jnp.abs(pre_act)))
-        turned = ebuf[j].T
+        turned = jnp.concatenate([ebuf[j]] + [jnp.zeros((-G % 8, R), F32)] * (G % 8 > 0), axis=0).T
         head_lane = lax.broadcasted_iota(jnp.int32, (1, turned.shape[1]), 1)
         add = jnp.sum(jnp.where(head_lane == i, turned, 0.0), axis=1, keepdims=True)
         logs[rows, :] = log_sig * (1.0 / 16.0) + add
 
-    if G > 1:
-        forward(1)
+    def kv_copy(slot, j):
+        part = kv.at[slot, pl.ds(pl.multiple_of(j * R, R), R)]
+        n = slot * G + j
+        return remote(part, part, kv_send.at[n], kv_recv.at[n], (sp + G, t))
+
+    def relay(step):
+        def one(s, _):
+            slot, j = o - s, source(step - s)
+            kv_copy(slot, j).wait_recv()
+
+            @pl.when(o < N - 1)
+            def _():
+                kv_copy(slot, j).start()
+
+            return 0
+
+        lax.fori_loop(jnp.maximum(1, step - G + 1), jnp.minimum(o, step) + 1, one, 0)
+
     for d in range(G):
         if 0 < d and d + 1 < G:
             forward(d + 1)
-        elif d == 0 and G > 1:
-            pass
         project(d)
 
-    def kv_copy(slot):
-        return remote(
-            kv.at[slot], kv.at[slot], kv_send.at[slot], kv_recv.at[slot], (sp + G, t)
-        )
-
-    @pl.when(o < N - 1)
-    def _():
-        kv_copy(o).start()
+        @pl.when(o < N - 1)
+        def _():
+            kv_copy(o, source(d)).start()
+
+        if d == 0 and G > 1:
+            forward(1)
+        relay(d)
 
     level_of = pair_level[...]
     states[...] = jnp.zeros_like(states)
@@ -304,30 +320,19 @@
 
         lax.fori_loop(0, 2 * S // TQ, tile, 0)
 
-    attend(o, True)
-
-    def take(slot):
-        kv_copy(slot).wait_recv()
-
-        @pl.when(o < N - 1)
-        def _():
-            kv_copy(slot).start()
-
-    @pl.when(o > 0)
-    def _():
-        take(o - 1)
-        prefix_copy().wait_recv()
-
-    @pl.when(o == 0)
-    def _():
-        pref_in[...] = jnp.zeros_like(pref_in)
-
-    carried = pref_in[...]
-
-    @pl.when(o < N - 1)
-    def _():
-        pref_out[...] = carried * jnp.exp(pre[G]) + states[G]
-        prefix_copy().start()
+    def give(n, ss, rs):
+        copies = []
+        for d in range(1, G):
+            j = lax.rem(i + d, G)
+            copies.append(
+                remote(obuf.at[n, j], mix.at[n, i], ss.at[d], rs.at[i], (peer(d), t))
+            )
+        return copies
+
+    def collect(n, ss, rs):
+        for d in range(1, G):
+            j = source(d)
+            remote(obuf.at[n, j], mix.at[n, j], ss.at[0], rs.at[j], (peer(1), t)).wait_recv()
 
     def chain_finish(b, _):
         rows = pl.ds(pl.multiple_of(b * R, R), R)
@@ -339,38 +344,40 @@
         obuf[1, b] = (full * lax.rsqrt(ms + RMS_EPS) * lgain[...] * gate).astype(BF16)
         return 0
 
-    lax.fori_loop(0, G, chain_finish, 0)
-
-    def give(n, ss, rs):
-        copies = []
-        for d in range(1, G):
-            j = lax.rem(i + d, G)
-            copies.append(
-                remote(obuf.at[n, j], mix.at[n, i], ss.at[d], rs.at[i], (peer(d), t))
-            )
-        for copy in copies:
+    def chain_tail():
+        @pl.when(o < N - 1)
+        def _():
+            pref_out[...] = pref_in[...] * jnp.exp(pre[G]) + states[G]
+            prefix_copy().start()
+
+        lax.fori_loop(0, G, chain_finish, 0)
+        for copy in give(1, c_send, c_recv):
             copy.start()
-        mix[n, i] = obuf[n, i]
-        return copies
-
-    def collect(n, ss, rs):
-        for d in range(1, G):
-            j = source(d)
-            remote(obuf.at[n, j], mix.at[n, j], ss.at[0], rs.at[j], (peer(1), t)).wait_recv()
-
-    sends += give(1, c_send, c_recv)
+        mix[1, i] = obuf[1, i]
+
+    @pl.when(o == 0)
+    def _():
+        pref_in[...] = jnp.zeros_like(pref_in)
+        chain_tail()
+
+    relay(G)
+    attend(o, True)
 
     def earlier(s, _):
-        slot = o - s
-
         @pl.when(s > 1)
         def _():
-            take(slot)
-
-        attend(slot, False)
+            relay(s + G - 1)
+
+        @pl.when(s == o)
+        def _():
+            prefix_copy().wait_recv()
+            chain_tail()
+
+        attend(o - s, False)
         return 0
 
     lax.fori_loop(1, o + 1, earlier, 0)
+    sends += give(1, c_send, c_recv)
 
     weight = lam[i]
 
@@ -384,7 +391,11 @@
         return 0
 
     lax.fori_loop(0, G, attn_finish, 0)
-    sends += give(0, a_send, a_recv)
+    attn_sends = give(0, a_send, a_recv)
+    for copy in attn_sends:
+        copy.start()
+    sends += attn_sends
+    mix[0, i] = obuf[0, i]
     for copy in wo_loads:
         copy.wait()
     collect(1, c_send, c_recv)
@@ -414,7 +425,8 @@
         prefix_copy().wait_send()
 
         def drain(s, _):
-            kv_copy(s).wait_send()
+            for j in range(G):
+                kv_copy(s, j).wait_send()
             return 0
 
         lax.fori_loop(0, o + 1, drain, 0)
@@ -437,7 +449,7 @@
     table, pair_level, levels = decay_tables(R)
     cfg = (G, N, T, r, R, S, D, LW, levels)
     row = lambda a: a.reshape(1, -1)
-    extra = jnp.pad(extra_shrinkage_exponent.T, ((0, -G % 8), (0, 0)))
+    extra = extra_shrinkage_exponent.T
     vmem = pl.BlockSpec(memory_space=pltpu.VMEM)
     smem = pl.BlockSpec(memory_space=pltpu.SMEM)
     anys = pl.BlockSpec(memory_space=pl.ANY)
@@ -479,8 +491,8 @@
             dma((G * T,)),
             dma((G,)),
             dma((G,)),
-            dma((N,)),
-            dma((N,)),
+            dma((N * G,)),
+            dma((N * G,)),
             dma((1,)),
             dma((1,)),
             dma((G,)),
@@ -496,9 +508,9 @@
         name="layer",
     )(
         tokens, row(input_norm_gain), differential_query, differential_key, differential_value,
-        linear_query, linear_key, linear_value, linear_output_gate, forget_down_factor,
+        linear_query, linear_key, linear_value, linear_output_gate, forget_down_factor.T,
         forget_up_factor, row(forget_bias), extra,
-        row(jnp.tile(query_norm_gain, 2)), row(jnp.tile(key_norm_gain, 2)), second_map_weight,
+        row(query_norm_gain), row(key_norm_gain), second_map_weight,
         row(differential_norm_gain), row(linear_norm_gain), differential_output_rows,
         linear_output_rows, jnp.asarray(table, BF16), jnp.asarray(pair_level),
     )

time: 62.4 us -> 50.7 us (0.81)
  Pallas kernels: 54.8 us -> 48.9 us
  local copies, waits for them, and re-layouts: 7.38 us -> 1.67 us
    pallas_call x1, Pallas kernels: 54.8 us -> 48.9 us  [per_device(): pl.pallas_call(functools.partial(body, cfg), out_shape=jax.ShapeDtypeStru...]
    another operation x4 -> x0, local copies, waits for them, and re-layouts: 2.53 us -> none  [the longest x2 1.22 us: per_device(): row = lambda a: a.reshape(1, -1)]
    unnamed x2 -> x1, local copies, waits for them, and re-layouts: 3.57 us -> 1.67 us
    pad x1 -> x0, local copies, waits for them, and re-layouts: 1.28 us -> none  [per_device(): extra = jnp.pad(extra_shrinkage_exponent.T, ((0, -G % 8), (0, 0)))]
where the time goes in v2:
time: 50.7 us; the launch traced here: 50.6 us
  Pallas kernels  48.9 us (96%)
  local copies, waits for them, and re-layouts  1.67 us (3%)
    pallas_call x1, Pallas kernels, per_device(): pl.pallas_call(functools.partial(body, cfg), out_shape=jax.ShapeDtypeStru...  48.9 us
    unnamed x1, local copies, waits for them, and re-layouts  1.67 us

profile of v2, /device:TPU:25, one launch (start us, length us, event | category | flops | bytes accessed | tf_op | source)
XLA Modules:
  0.0 50.6 jit_solution(15143526327063664276)
XLA Ops:
  0.0 48.9 %layer.1 = bf16[64,2048]{1,0:T(8,128)(2,1)} custom-call(bf16[64,2048]{1,0:T(8,128)(2,1)} %tokens.1, f32[1,2048]{1,0:T(1,128)} %bitcast.9, bf16[2048,512]{1,0:T(8,128)(2,1)} %wq.1, bf16[2048,512]{1,0:T(8,128)(2,1)} %wk.1, bf16[2048,512]{1,0:T(8,128)(2,1)} %wv.1, bf16[2048,256]{1,0:T(8,128)(2,1)} %wlq.1, bf16[2048,256]{1,0:T(8,128)(2,1)} %wlk.1, ...), custom_call_target="tpu_custom_call" | custom-call | tf_op jit(solution)/shard_map/layer/pallas_call | solution.py:458
  48.9 1.7 %copy.24 = bf16[64,2048]{1,0:T(8,128)(2,1)} copy(bf16[64,2048]{1,0:T(8,128)(2,1)} %layer.1) | data formatting | bytes 524288

commit v3 on v2

--- a/solution.py
+++ b/solution.py
@@ -252,7 +252,7 @@
     pre[...] = jnp.zeros_like(pre)
 
     def chain_block(b, _):
-        rows = pl.ds(pl.multiple_of(b * R, R), R)
+        rows = pl.ds(b * R, R)
         la = logs[rows, :]
         hi = la.astype(BF16)
         lo = (la - hi.astype(F32)).astype(BF16)
@@ -276,7 +276,8 @@
         pre[b + 1] = pre[b] + last
         return 0
 
-    lax.fori_loop(0, G, chain_block, 0)
+    for b in range(G):
+        chain_block(b, 0)
 
     def prefix_copy():
         return remote(
@@ -289,8 +290,7 @@
         k = kv.at[slot]
 
         def tile(j, _):
-            m = lax.div(j, S // TQ)
-            start = pl.multiple_of(lax.rem(j, S // TQ) * TQ, TQ)
+            m, start = j // (S // TQ), j % (S // TQ) * TQ
             rows = pl.ds(start, TQ)
             s = dot_t(q2[m, rows, :], k[:, 0:LANES])
             if first:
@@ -318,7 +318,8 @@
                 peak[m, rows, :] = new
             return 0
 
-        lax.fori_loop(0, 2 * S // TQ, tile, 0)
+        for j in range(2 * S // TQ):
+            tile(j, 0)
 
     def give(n, ss, rs):
         copies = []
@@ -335,7 +336,7 @@
             remote(obuf.at[n, j], mix.at[n, j], ss.at[0], rs.at[j], (peer(1), t)).wait_recv()
 
     def chain_finish(b, _):
-        rows = pl.ds(pl.multiple_of(b * R, R), R)
+        rows = pl.ds(b * R, R)
         state = (states[b] + pref_in[...] * jnp.exp(pre[b])).astype(BF16)
         full = inner[rows, :] + dot_t(qd[rows, :], state)
         gate = proj[rows, LANES : 2 * LANES].astype(F32)
@@ -350,7 +351,8 @@
             pref_out[...] = pref_in[...] * jnp.exp(pre[G]) + states[G]
             prefix_copy().start()
 
-        lax.fori_loop(0, G, chain_finish, 0)
+        for b in range(G):
+            chain_finish(b, 0)
         for copy in give(1, c_send, c_recv):
             copy.start()
         mix[1, i] = obuf[1, i]
@@ -382,7 +384,7 @@
     weight = lam[i]
 
     def attn_finish(b, _):
-        rows = pl.ds(pl.multiple_of(b * R, R), R)
+        rows = pl.ds(b * R, R)
         diff = acc[0, rows, :] / total[0, rows, :] - weight * (
             acc[1, rows, :] / total[1, rows, :]
         )
@@ -390,7 +392,8 @@
         obuf[0, b] = (diff * lax.rsqrt(ms + RMS_EPS) * dgain[...] * OUT_SCALE).astype(BF16)
         return 0
 
-    lax.fori_loop(0, G, attn_finish, 0)
+    for b in range(G):
+        attn_finish(b, 0)
     attn_sends = give(0, a_send, a_recv)
     for copy in attn_sends:
         copy.start()

time: 50.7 us -> 47.9 us (0.945)
  Pallas kernels: 48.9 us -> 46.1 us
    pallas_call x1, Pallas kernels: 48.9 us -> 46.1 us  [per_device(): pl.pallas_call(functools.partial(body, cfg), out_shape=jax.ShapeDtypeStru...]
where the time goes in v3:
time: 47.9 us; the launch traced here: 47.8 us
  Pallas kernels  46.1 us (96%)
  local copies, waits for them, and re-layouts  1.67 us (3%)
    pallas_call x1, Pallas kernels, per_device(): pl.pallas_call(functools.partial(body, cfg), out_shape=jax.ShapeDtypeStru...  46.1 us
    unnamed x1, local copies, waits for them, and re-layouts  1.67 us

profile of v3, /device:TPU:25, one launch (start us, length us, event | category | flops | bytes accessed | tf_op | source)
XLA Modules:
  0.0 47.8 jit_solution(2433352800937766405)
XLA Ops:
  0.0 46.1 %layer.1 = bf16[64,2048]{1,0:T(8,128)(2,1)} custom-call(bf16[64,2048]{1,0:T(8,128)(2,1)} %tokens.1, f32[1,2048]{1,0:T(1,128)} %bitcast.9, bf16[2048,512]{1,0:T(8,128)(2,1)} %wq.1, bf16[2048,512]{1,0:T(8,128)(2,1)} %wk.1, bf16[2048,512]{1,0:T(8,128)(2,1)} %wv.1, bf16[2048,256]{1,0:T(8,128)(2,1)} %wlq.1, bf16[2048,256]{1,0:T(8,128)(2,1)} %wlk.1, ...), custom_call_target="tpu_custom_call" | custom-call | tf_op jit(solution)/shard_map/layer/pallas_call | solution.py:461
  46.1 1.7 %copy.24 = bf16[64,2048]{1,0:T(8,128)(2,1)} copy(bf16[64,2048]{1,0:T(8,128)(2,1)} %layer.1) | data formatting | bytes 524288
